TPU v7x, 256 devices: a 4x2x16 block of a 4x16x16 slice. The times are simulated.
256 devices in a mesh: grp: 2 (over y), sp: 32 (over z, core), tp: 4 (over x).
Axes of the slice: x: 4, y: 2, z: 16, core: 2. Of those that a mesh axis runs over, the one named last changes fastest.
The devices are a block of a 4x16x16 slice.
Arguments:
- stream_in: bfloat16 [32768, 2048], P(('grp', 'sp')), parts along dimension 0, may hold values from -6 to 6
- query_wide: bfloat16 [32768, 1024], P(('grp', 'sp'), 'tp'), parts along dimension 0, may hold values from -6 to 6
- key_wide: bfloat16 [32768, 1024], P(('grp', 'sp'), 'tp'), parts along dimension 0, may hold values from -6 to 6
- value_wide: bfloat16 [32768, 2048], P(('grp', 'sp'), 'tp'), parts along dimension 0, may hold values from -6 to 6
- query_narrow: bfloat16 [32768, 512], P(('grp', 'sp'), 'tp'), parts along dimension 0, may hold values from -6 to 6
- key_narrow: bfloat16 [32768, 512], P(('grp', 'sp'), 'tp'), parts along dimension 0, may hold values from -6 to 6
- value_narrow: bfloat16 [32768, 1024], P(('grp', 'sp'), 'tp'), parts along dimension 0, may hold values from -6 to 6
- decay_wide: float32 [4, 32768], P('tp', ('grp', 'sp')), parts along dimension 1, may hold values from -1 to 0
- decay_narrow: float32 [4, 32768], P('tp', ('grp', 'sp')), parts along dimension 1, may hold values from -1 to 0
- gain_wide: float32 [2048], P('tp'), may hold values from 0.1 to 1.9
- gain_narrow: float32 [1024], P('tp'), may hold values from 0.1 to 1.9
- out_wide: bfloat16 [2048, 2048], P('tp'), may hold values from -0.109375 to 0.109375
- out_narrow: bfloat16 [1024, 2048], P('tp'), may hold values from -0.109375 to 0.109375
- mlp_gain: float32 [2048], replicated, may hold values from 0.1 to 1.9
- up_weight: bfloat16 [2048, 8192], P('sp', 'tp'), may hold values from -0.125 to 0.125
- down_weight: bfloat16 [8192, 2048], P('tp', 'sp'), may hold values from -0.0625 to 0.0625
Outputs:
- stream_out: bfloat16 [32768, 2048], P(('grp', 'sp', 'tp')), parts along dimension 0
There are 2 independent parts, one for each index of `grp`. A program takes and returns all parts, laid end to end along the dimension named above; an argument that names none is the same for every part. Nothing has to cross between parts.
All inputs are finite; a program needn't handle non-finite values.
Results may differ from a plain program's by a relative error of at most 0.019.
Values may be sent and summed in bfloat16 or wider, within the bound.
No kernel may reach another device: no remote copies, remote signals or barrier semaphores. Data moves between devices by JAX's collectives and lax.ppermute only.
A program may use at most 128 MiB of HBM per device.

v0:
```python
import jax
import jax.numpy as jnp
from jax import lax
from jax.sharding import Mesh
from jax.sharding import PartitionSpec as P

SP = ("sp_0", "sp_1")
GRP_SP = ("grp", "sp_0", "sp_1")
GRP_SP_TP = ("grp", "sp_0", "sp_1", "tp")
EPS = 1e-06


def neutral_like(x, identity):
    return jax.tree.map(
        lambda a, e: jnp.broadcast_to(jnp.asarray(e, a.dtype), a.shape), x, identity
    )


def entering(x, axes, combine, identity):
    before = start = neutral_like(x, identity)
    total = x
    for axis in reversed(axes):
        length, mine = (lax.axis_size(axis), lax.axis_index(axis))
        pieces = jax.tree.map(
            lambda part, kind: lax.all_gather(part.astype(kind), axis),
            total,
            (jnp.bfloat16, jnp.bfloat16, jnp.bfloat16, jnp.bfloat16),
        )
        inside, total = (start, start)
        for k in range(length):
            passed = k < mine
            total = combine(
                total, jax.tree.map(lambda part, own: part[k].astype(own.dtype), pieces, x)
            )
            inside = jax.tree.map(lambda new, old: jnp.where(passed, new, old), total, inside)
        before = combine(inside, before)
    return before


def rows_first(arrays, axis, dims):
    turned = [jnp.moveaxis(a, dim, 0) for a, dim in zip(arrays, dims)]
    both = jnp.concatenate([t.reshape(len(t), -1) for t in turned], axis=1)
    result, at, done = (lax.all_gather(both, axis, axis=0, tiled=True), 0, [])
    for t, dim in zip(turned, dims):
        slab = result[:, at : at + t[0].size].reshape(-1, *t.shape[1:])
        done.append(jnp.moveaxis(slab, 0, dim))
        at += t[0].size
    return tuple(done)


def split_up(x, dim, length):
    before, after = (x.shape[:dim], x.shape[dim + 1 :])
    return jnp.moveaxis(x.reshape(*before, length, -1, *after), dim, 0)


def summed_on_arrival(x, axis, dim):
    parts = split_up(x, dim, lax.axis_size(axis))
    arrived = lax.all_to_all(parts, axis, split_axis=0, concat_axis=0, tiled=True)
    return arrived.astype(jnp.float32).sum(axis=0)


def joined_along(parts, dim):
    parts = jnp.moveaxis(parts, 0, dim)
    lengths = parts.shape
    return parts.reshape(*lengths[:dim], lengths[dim] * lengths[dim + 1], *lengths[dim + 2 :])


def copy_for_each(x, axis):
    length = lax.axis_size(axis)
    return lax.all_to_all(jnp.broadcast_to(x[None], (length, *x.shape)), axis, 0, 0, tiled=True)


def collect(x, axis, dim):
    return joined_along(copy_for_each(x, axis), dim)


def retain_local(queries, key_rows, value_rows, log_decay):
    total_heads = log_decay.shape[0]
    length = queries.shape[0]
    key_width = queries.shape[1] // total_heads
    value_width = value_rows.shape[1] // total_heads
    query_heads = queries.reshape(length, total_heads, key_width)
    key_heads = key_rows.reshape(length, total_heads, key_width)
    value_heads = value_rows.reshape(length, total_heads, value_width)
    cumulative = jnp.cumsum(log_decay, axis=1)
    row_index = lax.broadcasted_iota(jnp.int32, (length, length), 0)
    col_index = lax.broadcasted_iota(jnp.int32, (length, length), 1)
    causal = (row_index >= col_index)[None]
    log_gap = cumulative[:, :, None] - cumulative[:, None, :]
    fading = jnp.where(causal, jnp.exp(jnp.where(causal, log_gap, 0.0)), 0.0)
    scores = jnp.einsum("ihd,jhd->hij", query_heads, key_heads, preferred_element_type=jnp.float32)
    weights_low = (scores * key_width ** (-0.5) * fading).astype(jnp.bfloat16)
    within = jnp.einsum(
        "hij,jhe->ihe", weights_low, value_heads, preferred_element_type=jnp.float32
    )
    to_end = jnp.exp(cumulative[:, -1:] - cumulative)
    keyed = (key_heads.astype(jnp.float32) * key_width ** (-0.5) * to_end.T[:, :, None]).astype(
        jnp.bfloat16
    )
    local_state = jnp.einsum("jhd,jhe->hde", keyed, value_heads, preferred_element_type=jnp.float32)
    overall = jnp.exp(cumulative[:, -1])
    return (query_heads, cumulative, within, overall, local_state)


def finish(query_heads, cumulative, within, incoming, gain_values):
    carried = (
        jnp.einsum(
            "ihd,hde->ihe",
            query_heads.astype(jnp.float32),
            incoming,
            precision=lax.Precision.HIGHEST,
        )
        * jnp.exp(cumulative).T[:, :, None]
    )
    retained = within + carried
    centered = retained - jnp.mean(retained, axis=-1, keepdims=True)
    scaled = centered * lax.rsqrt(jnp.mean(centered * centered, axis=-1, keepdims=True) + EPS)
    return (scaled.reshape(retained.shape[0], -1) * gain_values).astype(jnp.bfloat16)


def normalize(rows, gain_values):
    values = rows.astype(jnp.float32)
    scaled = values * lax.rsqrt(jnp.mean(values * values, axis=-1, keepdims=True) + EPS)
    return (scaled * gain_values).astype(jnp.bfloat16)


def join_states(earlier, latter):
    return (
        earlier[0] * latter[0],
        latter[0][:, None, None] * earlier[1] + latter[1],
        earlier[2] * latter[2],
        latter[2][:, None, None] * earlier[3] + latter[3],
    )


def on_device(
    stream_in,
    query_wide,
    key_wide,
    value_wide,
    query_narrow,
    key_narrow,
    value_narrow,
    decay_wide,
    decay_narrow,
    gain_wide,
    gain_narrow,
    out_wide,
    out_narrow,
    mlp_gain,
    up_weight,
    down_weight,
):
    length = stream_in.shape[0]
    portion = length // lax.axis_size("tp")
    member = lax.axis_index("tp")
    wide_query, wide_cum, wide_within, wide_factor, wide_state = retain_local(
        query_wide, key_wide, value_wide, decay_wide
    )
    thin_query, thin_cum, thin_within, thin_factor, thin_state = retain_local(
        query_narrow, key_narrow, value_narrow, decay_narrow
    )
    identity = (
        jnp.ones_like(wide_factor),
        jnp.zeros_like(wide_state),
        jnp.ones_like(thin_factor),
        jnp.zeros_like(thin_state),
    )
    incoming = entering(
        (wide_factor, wide_state, thin_factor, thin_state), SP, join_states, identity
    )
    normed_wide = finish(wide_query, wide_cum, wide_within, incoming[1], gain_wide)
    normed_thin = finish(thin_query, thin_cum, thin_within, incoming[3], gain_narrow)
    up_full, down_full = rows_first((up_weight, down_weight), SP, (0, 1))
    mixed_heads = summed_on_arrival(
        (
            jnp.dot(normed_wide, out_wide, preferred_element_type=jnp.float32)
            + jnp.dot(normed_thin, out_narrow, preferred_element_type=jnp.float32)
        ).astype(jnp.bfloat16),
        "tp",
        0,
    )
    own_stream = lax.dynamic_slice_in_dim(stream_in, member * portion, portion, 0)
    middle = (own_stream.astype(jnp.float32) + mixed_heads).astype(jnp.bfloat16)
    raised = jax.nn.relu(
        jnp.dot(
            collect(normalize(middle, mlp_gain), "tp", 0),
            up_full,
            preferred_element_type=jnp.float32,
        )
    )
    hidden = (raised * raised).astype(jnp.bfloat16)
    channel = summed_on_arrival(
        jnp.dot(hidden, down_full, preferred_element_type=jnp.float32).astype(jnp.bfloat16), "tp", 0
    )
    return (middle.astype(jnp.float32) + channel).astype(jnp.bfloat16)


def solution(mesh):
    torus = Mesh(
        mesh.devices.reshape(mesh.shape["grp"], 16, 2, mesh.shape["tp"]),
        ("grp", "sp_0", "sp_1", "tp"),
    )
    placed = (
        P(GRP_SP, None),
        P(GRP_SP, "tp"),
        P(GRP_SP, "tp"),
        P(GRP_SP, "tp"),
        P(GRP_SP, "tp"),
        P(GRP_SP, "tp"),
        P(GRP_SP, "tp"),
        P("tp", GRP_SP),
        P("tp", GRP_SP),
        P("tp"),
        P("tp"),
        P("tp", None),
        P("tp", None),
        P(),
        P(SP, "tp"),
        P("tp", SP),
    )
    return jax.shard_map(
        on_device, mesh=torus, in_specs=placed, out_specs=P(GRP_SP_TP, None), check_vma=False
    )
```

profile of v0, /device:TPU:33, one launch (start us, length us, event | category | flops | bytes accessed | tf_op | source)
XLA Modules:
  0.0 342.9 jit_solution(9512883190763255492)
XLA Ops:
  6.5 0.0 copy-start
  6.6 0.1 all-gather.10.cloned.1.call-start
  6.6 1.1 reduce-window.14
  7.8 0.2 slice_reduce_fusion.1
  7.9 0.2 reduce-window.15
  8.1 0.1 broadcast.496
  8.2 0.7 slice.363
  8.9 0.6 slice.362
  10.8 1.0 reduce-window.16
  11.8 0.2 slice_reduce_fusion
  11.9 0.2 reduce-window.19
  12.1 0.1 broadcast.499
  12.2 0.6 slice.383
  12.8 0.6 slice.382
  14.6 0.1 exponential_multiply_fusion
  14.7 1.3 dynamic-slice
  16.0 0.8 dynamic-update-slice
  16.7 0.8 dynamic-update-slice.2
  17.5 1.4 convolution_convert_fusion.1
  18.9 22.0 %all-gather.3 = bf16[256,256]{1,0:T(8,128)(2,1)S(1)} all-gather(bf16[128,256]{1,0:T(8,128)(2,1)S(1)} %convolution_convert_fusion.1), channel_id=5, replica_groups=mesh['grp'=2,'sp_0'=16,'sp_1'=2,'tp'=4] {'sp_1'}, dimensions={0}, use_global_device_ids=true | all-gather | bytes 196608 | tf_op jit(solution)/shard_map/all_gather | solution.py:25
  40.9 2.5 all-reduce.5
  43.4 0.6 slice_convert_fusion.1
  44.6 1.3 fusion.248
  45.8 0.1 all-gather.10.cloned.1.call-update
  45.9 0.1 all-gather.8.cloned.1.call-start
  46.6 0.1 exponential_multiply_fusion.1
  46.7 1.5 convolution_convert_fusion
  48.3 2.2 all-gather.1
  50.5 1.4 fusion.115
  51.9 0.1 all-gather.8.cloned.1.call-update
  52.0 0.1 all-gather.12.cloned.1.call-start
  52.1 0.0 copy-done.4
  52.1 0.0 copy-done.5
  52.1 0.8 pad_maximum_fusion
  52.9 0.1 all-gather.12.cloned.1.call-update
  53.0 1.3 dynamic-slice.1
  54.3 0.7 fusion.317
  54.9 1.3 dynamic-update-slice.1
  56.3 1.3 dynamic-update-slice.3
  57.6 24.1 %all-reduce.4 = (bf16[16]{0:T(256)(128)(2,1)S(1)}, bf16[16]{0:T(256)(128)(2,1)S(1)}) all-reduce(bf16[16]{0:T(256)(128)(2,1)S(1)} %dynamic-update-slice.1, bf16[16]{0:T(256)(128)(2,1)S(1)} %dynamic-update-slice.3), channel_id=2, replica_groups=mesh['grp'=2,'sp_0'=16,'sp_1'=2,'tp'=4] {'sp_0'}, use_global_device_ids=true, to_apply=%add.1 | all-reduce | flops 32 | bytes 128
  82.9 0.7 fusion.315
  93.6 0.7 fusion.316
  105.6 2.3 fusion.18
  107.9 3.0 convolution_bitcast_fusion.1
  111.0 3.0 fusion.319
  114.0 0.1 multiply_reduce_fusion.1
  114.2 2.8 fusion.116
  117.0 58.9 %all-gather.8.cloned.1.call-done = bf16[16,1,256,512]{3,2,1,0:T(8,128)(2,1)} async-done(((bf16[1,1,256,512]{3,2,1,0:T(8,128)(2,1)}), bf16[16,1,256,512]{3,2,1,0:T(8,128)(2,1)}) %all-gather.8.cloned.1.call-update) | async-done | bytes 4194320 | tf_op jit(solution)/shard_map/all_gather | solution.py:25
  175.9 0.0 copy-done.9
  175.9 6.0 %fusion.320 = (f32[512]{0:T(512)S(1)}, f32[1,512,512]{2,1,0:T(8,128)S(1)}) fusion(f32[1,512,512]{2,1,0:T(8,128)} %convolution_bitcast_fusion.1, f32[512]{0:T(512)S(1)} %exp.55, bf16[512,256]{1,0:T(8,128)(2,1)S(1)} %copy-done.9, bf16[16,1,256,512]{3,2,1,0:T(8,128)(2,1)} %all-gather.8.cloned.1.call-done, f32[]{:T(128)} %bitcast.30, f32[]{:T(128)} %bitcast.31, ...), kind=kOutput, calls=%fused_computation.358 | convolution fusion | flops 815529472 | bytes 7082078 | tf_op jit(solution)/shard_map/ihd,hde->ihe/dot_general | solution.py:107
  181.8 0.2 multiply_reduce_fusion
  182.1 2.8 add_convert_fusion
  184.9 4.7 %all-to-all-start = ((bf16[4,128,2048]{2,1,0:T(8,128)(2,1)}), bf16[4,128,2048]{2,1,0:T(8,128)(2,1)}, u32[]{:S(2)}, u32[]{:S(2)}) async-start(bf16[4,128,2048]{2,1,0:T(8,128)(2,1)} %bitcast.179), calls=%async_computation | async-start | bytes 4194304 | tf_op jit(solution)/shard_map/all_to_all | solution.py:58
  189.5 16.5 %all-to-all-done = bf16[4,128,2048]{2,1,0:T(8,128)(2,1)} async-done(((bf16[4,128,2048]{2,1,0:T(8,128)(2,1)}), bf16[4,128,2048]{2,1,0:T(8,128)(2,1)}, u32[]{:S(2)}, u32[]{:S(2)}) %all-to-all-start) | async-done | bytes 2097184 | tf_op jit(solution)/shard_map/all_to_all | solution.py:58
  206.0 2.1 convert_reduce_fusion.1
  208.1 1.4 fusion.21
  209.5 0.2 fusion.23
  209.7 0.2 broadcast_in_dim.16
  209.9 18.6 %all_to_all.15 = bf16[4,128,2048]{2,1,0:T(8,128)(2,1)} all-to-all(bf16[4,128,2048]{2,1,0:T(8,128)(2,1)S(1)} %broadcast_in_dim.16), channel_id=1, replica_groups=mesh['grp'=2,'sp_0'=16,'sp_1'=2,'tp'=4] {'tp'}, dimensions={0} | all-to-all | bytes 4194304 | tf_op jit(solution)/shard_map/all_to_all | solution.py:70
  228.5 60.1 %all-gather.12.cloned.1.call-done = bf16[2048,4096]{1,0:T(8,128)(2,1)} async-done(((bf16[64,4096]{1,0:T(8,128)(2,1)}), bf16[2048,4096]{1,0:T(8,128)(2,1)}) %all-gather.12.cloned.1.call-update) | async-done | bytes 16777232 | tf_op jit(solution)/shard_map/all_gather | solution.py:43
  288.7 16.5 %fusion.6 = bf16[512,2048]{1,0:T(8,128)(2,1)} fusion(bf16[2048,4096]{1,0:T(8,128)(2,1)} %all-gather.12.cloned.1.call-done, bf16[512,2048]{1,0:T(8,128)(2,1)} %bitcast.180), kind=kOutput, calls=%fused_computation.8 | convolution fusion | flops 8594128896 | bytes 20971520 | tf_op jit(solution)/shard_map/dot_general | solution.py:194
  305.2 29.9 %all_to_all.16 = bf16[4,128,2048]{2,1,0:T(8,128)(2,1)S(1)} all-to-all(bf16[4,128,2048]{2,1,0:T(8,128)(2,1)} %bitcast.181), channel_id=1, replica_groups=mesh['grp'=2,'sp_0'=16,'sp_1'=2,'tp'=4] {'tp'}, dimensions={0} | all-to-all | bytes 4194304 | tf_op jit(solution)/shard_map/all_to_all | solution.py:58
  335.0 0.4 convert_reduce_fusion
  335.4 0.9 fusion.24
  (30 shorter events, 0.1 us)
Async XLA Ops:
  6.5 175.5 %copy-start = (bf16[512,2048]{1,0:T(8,128)(2,1)S(1)}, bf16[512,2048]{1,0:T(8,128)(2,1)}, u32[]{:S(2)}) copy-start(bf16[512,2048]{1,0:T(8,128)(2,1)} %param.27) | copy-start | bytes 6291460
  6.6 99.0 %copy-start.3 = (bf16[512,256]{1,0:T(8,128)(2,1)S(1)}, bf16[512,256]{1,0:T(8,128)(2,1)}, u32[]{:S(2)}) copy-start(bf16[512,256]{1,0:T(8,128)(2,1)} %param.22) | copy-start | bytes 786436
  6.6 45.5 %copy-start.4 = (bf16[2048,64]{0,1:T(8,128)(2,1)S(1)}, bf16[2048,64]{0,1:T(8,128)(2,1)}, u32[]{:S(2)}) copy-start(bf16[2048,64]{0,1:T(8,128)(2,1)} %param.31) | copy-start | bytes 786436
  6.6 45.5 %copy-start.5 = (bf16[64,2048]{1,0:T(8,128)(2,1)S(1)}, bf16[64,2048]{1,0:T(8,128)(2,1)}, u32[]{:S(2)}) copy-start(bf16[64,2048]{1,0:T(8,128)(2,1)} %param.30) | copy-start | bytes 786436
  6.6 104.4 %all-gather.10.cloned.1.call-start = ((), (), s32[]{:S(2)}) async-start(), calls=%async_computation.4 | async-start | bytes 1114112 | tf_op jit(solution)/shard_map/all_gather | solution.py:25
  45.9 130.0 %all-gather.8.cloned.1.call-start = ((), (), s32[]{:S(2)}) async-start(), calls=%async_computation.3 | async-start | bytes 4456448 | tf_op jit(solution)/shard_map/all_gather | solution.py:25
  52.0 236.7 %all-gather.12.cloned.1.call-start = ((), (), s32[]{:S(2)}) async-start(), calls=%async_computation.5 | async-start | bytes 17301504 | tf_op jit(solution)/shard_map/all_gather | solution.py:43
  107.9 6.2 %copy-start.7 = (f32[256]{0:T(256)S(1)}, f32[256]{0:T(256)}, u32[]{:S(2)}) copy-start(f32[256]{0:T(256)} %param.26) | copy-start | bytes 3076
  111.0 3.2 copy-start.2
  114.1 61.7 %copy-start.9 = (bf16[512,256]{1,0:T(8,128)(2,1)S(1)}, bf16[512,256]{1,0:T(8,128)(2,1)}, u32[]{:S(2)}) copy-start(bf16[512,256]{1,0:T(8,128)(2,1)} %param.17) | copy-start | bytes 786436
  175.9 6.2 %copy-start.1 = (f32[512,2048]{1,0:T(8,128)S(1)}, f32[512,2048]{1,0:T(8,128)}, u32[]{:S(2)}) copy-start(f32[512,2048]{1,0:T(8,128)} %fusion.116) | copy-start | bytes 12582916
  175.9 6.2 %copy-start.8 = (f32[512]{0:T(512)S(1)}, f32[512]{0:T(512)}, u32[]{:S(2)}) copy-start(f32[512]{0:T(512)} %param.25) | copy-start | bytes 6148
  184.9 24.6 %copy-start.6 = (f32[2048]{0:T(1024)S(1)}, f32[2048]{0:T(1024)}, u32[]{:S(2)}) copy-start(f32[2048]{0:T(1024)} %param.29) | copy-start | bytes 24580
  184.9 21.1 %all-to-all-start = ((bf16[4,128,2048]{2,1,0:T(8,128)(2,1)}), bf16[4,128,2048]{2,1,0:T(8,128)(2,1)}, u32[]{:S(2)}, u32[]{:S(2)}) async-start(bf16[4,128,2048]{2,1,0:T(8,128)(2,1)} %bitcast.179), calls=%async_computation | async-start | bytes 4194304 | tf_op jit(solution)/shard_map/all_to_all | solution.py:58
Sparse Core Ops, SparseCore 0:
  46.0 52.9 all-gather.9
  100.8 74.9 all-gather.7
  177.7 110.9 all-gather.11
where the time goes:
time: 344 us; the launch traced here: 343 us
  waiting for transfers between devices  136 us (40%)
  blocking collectives  99.3 us (29%)
  between operations  39.6 us (12%)
  matrix products  39.3 us (11%)
  other arithmetic  12.7 us (4%)
  local copies, waits for them, and re-layouts  11.4 us (3%)
  starting transfers between devices  4.84 us (1%)
    all_gather x1, waiting for transfers between devices, rows_first(): result, at, done = (lax.all_gather(both, axis, axis=0, tiled=True), 0, [])  60.1 us
    all_gather x2, waiting for transfers between devices, entering(): lax.all_gather(part.astype(kind), axis)  58.9 us
    all_to_all x1, blocking collectives, summed_on_arrival(): lax.all_to_all(parts, axis, split_axis=0, concat_axis=0, tiled=True)  29.9 us
    unnamed x2, blocking collectives  26.6 us
    all_gather x2, blocking collectives, entering(): lax.all_gather(part.astype(kind), axis)  24.2 us
    all_to_all x1, blocking collectives, copy_for_each(): lax.all_to_all(jnp.broadcast_to(x[None], (length, *x.shape)), axis, 0, 0,...  18.6 us
    dot_general x1, matrix products, on_device(): jnp.dot(hidden, down_full, preferred_element_type=jnp.float32)  16.5 us
    all_to_all x1, waiting for transfers between devices, summed_on_arrival(): lax.all_to_all(parts, axis, split_axis=0, concat_axis=0, tiled=True)  16.5 us
  transfers between devices with their start and end apart: 4, of which 3 were waited for; matrix products, arithmetic and copies ran while one was open for 10% of the time, Pallas kernels for 0%

commit v1 on v0

--- a/solution.py
+++ b/solution.py
@@ -8,6 +8,11 @@
 GRP_SP = ("grp", "sp_0", "sp_1")
 GRP_SP_TP = ("grp", "sp_0", "sp_1", "tp")
 EPS = 1e-06
+
+
+def all_by_exchange(x, mesh_axis, along):
+    sent = jnp.stack([x] * lax.axis_size(mesh_axis))
+    return jnp.concatenate(lax.all_to_all(sent, mesh_axis, 0, 0), axis=along)
 
 
 def neutral_like(x, identity):
@@ -40,7 +45,7 @@
 def rows_first(arrays, axis, dims):
     turned = [jnp.moveaxis(a, dim, 0) for a, dim in zip(arrays, dims)]
     both = jnp.concatenate([t.reshape(len(t), -1) for t in turned], axis=1)
-    result, at, done = (lax.all_gather(both, axis, axis=0, tiled=True), 0, [])
+    result, at, done = (all_by_exchange(both, axis, 0), 0, [])
     for t, dim in zip(turned, dims):
         slab = result[:, at : at + t[0].size].reshape(-1, *t.shape[1:])
         done.append(jnp.moveaxis(slab, 0, dim))

time: 344 us -> 1040 us (3.02)
  blocking collectives: 99.3 us -> 830 us
  waiting for transfers between devices: 136 us -> 90.5 us
    all_to_all x1, blocking collectives: 18.6 us -> 749 us  [all_by_exchange(): return jnp.concatenate(lax.all_to_all(sent, mesh_axis, 0, 0), axis=along)]
    all_gather x1 -> x0, waiting for transfers between devices: 60.1 us -> none  [rows_first(): result, at, done = (lax.all_gather(both, axis, axis=0, tiled=True), 0, [])]
    all_to_all x0 -> x1, waiting for transfers between devices: none -> 15.3 us  [copy_for_each(): lax.all_to_all(jnp.broadcast_to(x[None], (length, *x.shape)), axis, 0, 0,...]
  transfers between devices with their start and end apart: 4 -> 4, of which waited for: 3 -> 3; matrix products, arithmetic and copies ran while one was open for 10% -> 2% of each run, Pallas kernels for 0% -> 0%
where the time goes in v1:
time: 1040 us; the launch traced here: 1030 us
  blocking collectives  830 us (80%)
  waiting for transfers between devices  90.5 us (9%)
  between operations  40.4 us (4%)
  matrix products  39.3 us (4%)
  local copies, waits for them, and re-layouts  14.7 us (1%)
    all_to_all x1, blocking collectives, all_by_exchange(): return jnp.concatenate(lax.all_to_all(sent, mesh_axis, 0, 0), axis=along)  749 us
    all_gather x2, waiting for transfers between devices, entering(): lax.all_gather(part.astype(kind), axis)  58.9 us
    all_to_all x1, blocking collectives, summed_on_arrival(): lax.all_to_all(parts, axis, split_axis=0, concat_axis=0, tiled=True)  29.7 us
    unnamed x2, blocking collectives  27.2 us
    all_gather x2, blocking collectives, entering(): lax.all_gather(part.astype(kind), axis)  24.2 us
  transfers between devices with their start and end apart: 4, of which 3 were waited for; matrix products, arithmetic and copies ran while one was open for 2% of the time, Pallas kernels for 0%

profile of v1, /device:TPU:33, one launch (start us, length us, event | category | flops | bytes accessed | tf_op | source)
XLA Modules:
  0.0 1033.9 jit_solution(7052849535006086324)
XLA Ops:
  6.5 0.0 copy-start
  6.6 0.1 all-gather.9.cloned.1.call-start
  6.6 1.1 reduce-window.16
  7.8 0.2 slice_reduce_fusion
  7.9 0.6 slice.382
  8.5 0.2 reduce-window.19
  8.7 0.1 broadcast.501
  8.8 0.7 slice.383
  10.8 0.1 exponential_multiply_fusion
  10.9 1.0 reduce-window.14
  11.9 0.2 slice_reduce_fusion.1
  12.1 0.6 slice.362
  12.7 0.2 reduce-window.15
  12.9 0.1 broadcast.498
  12.9 0.6 slice.363
  14.8 1.3 dynamic-slice
  16.0 0.7 dynamic-update-slice
  16.7 0.7 dynamic-update-slice.2
  17.4 1.4 convolution_convert_fusion.1
  18.7 22.0 %all-gather.3 = bf16[256,256]{1,0:T(8,128)(2,1)S(1)} all-gather(bf16[128,256]{1,0:T(8,128)(2,1)S(1)} %convolution_convert_fusion.1), channel_id=5, replica_groups=mesh['grp'=2,'sp_0'=16,'sp_1'=2,'tp'=4] {'sp_1'}, dimensions={0}, use_global_device_ids=true | all-gather | bytes 196608 | tf_op jit(solution)/shard_map/all_gather | solution.py:30
  40.8 2.5 all-reduce.5
  43.2 0.7 slice_convert_fusion.1
  44.5 1.3 fusion.248
  45.7 0.1 all-gather.9.cloned.1.call-update
  45.8 0.1 all-gather.7.cloned.1.call-start
  46.6 0.1 exponential_multiply_fusion.1
  46.6 1.5 convolution_convert_fusion
  48.2 2.2 all-gather.1
  50.4 1.5 fusion.115
  51.9 0.1 all-gather.7.cloned.1.call-update
  52.0 1.3 dynamic-slice.1
  53.3 0.7 fusion.317
  54.0 1.4 dynamic-update-slice.1
  55.4 1.4 dynamic-update-slice.3
  56.8 24.8 %all-reduce.4 = (bf16[16]{0:T(256)(128)(2,1)S(1)}, bf16[16]{0:T(256)(128)(2,1)S(1)}) all-reduce(bf16[16]{0:T(256)(128)(2,1)S(1)} %dynamic-update-slice.1, bf16[16]{0:T(256)(128)(2,1)S(1)} %dynamic-update-slice.3), channel_id=2, replica_groups=mesh['grp'=2,'sp_0'=16,'sp_1'=2,'tp'=4] {'sp_0'}, use_global_device_ids=true, to_apply=%add.1 | all-reduce | flops 32 | bytes 128
  82.8 0.7 fusion.316
  93.7 0.7 fusion.315
  105.8 0.0 copy-done.4
  105.8 0.0 copy-done.7
  105.9 2.3 fusion.18
  108.1 2.9 convolution_bitcast_fusion.1
  111.1 3.0 fusion.319
  114.1 0.1 multiply_reduce_fusion.1
  114.3 2.8 fusion.116
  117.1 58.9 %all-gather.7.cloned.1.call-done = bf16[16,1,256,512]{3,2,1,0:T(8,128)(2,1)} async-done(((bf16[1,1,256,512]{3,2,1,0:T(8,128)(2,1)}), bf16[16,1,256,512]{3,2,1,0:T(8,128)(2,1)}) %all-gather.7.cloned.1.call-update) | async-done | bytes 4194320 | tf_op jit(solution)/shard_map/all_gather | solution.py:30
  175.9 6.0 fusion.320
  182.0 0.2 multiply_reduce_fusion
  182.2 0.0 copy-done
  182.2 2.8 add_convert_fusion
  185.0 4.1 all-to-all-start
  189.2 16.2 %all-to-all-done = bf16[4,128,2048]{2,1,0:T(8,128)(2,1)S(1)} async-done(((bf16[4,128,2048]{2,1,0:T(8,128)(2,1)}), bf16[4,128,2048]{2,1,0:T(8,128)(2,1)S(1)}, u32[]{:S(2)}, u32[]{:S(2)}) %all-to-all-start) | async-done | bytes 2097184 | tf_op jit(solution)/shard_map/all_to_all | solution.py:63
  205.4 0.4 convert_reduce_fusion.1
  205.7 1.3 fusion.21
  207.0 0.0 copy-start.6
  207.1 0.2 fusion.23
  207.3 1.6 broadcast_in_dim.16
  208.9 4.5 all-to-all-start.1
  213.5 15.3 %all-to-all-done.1 = bf16[4,128,2048]{2,1,0:T(8,128)(2,1)} async-done(((bf16[4,128,2048]{2,1,0:T(8,128)(2,1)}), bf16[4,128,2048]{2,1,0:T(8,128)(2,1)}, u32[]{:S(2)}, u32[]{:S(2)}) %all-to-all-start.1) | async-done | bytes 2097184 | tf_op jit(solution)/shard_map/all_to_all | solution.py:75
  228.8 1.9 stack.2
  230.7 748.8 %all_to_all.20 = bf16[32,64,4096]{2,1,0:T(8,128)(2,1)} all-to-all(bf16[32,64,4096]{2,1,0:T(8,128)(2,1)S(1)} %stack.2), channel_id=1, replica_groups=mesh['grp'=2,'sp_0'=16,'sp_1'=2,'tp'=4] {'sp_0','sp_1'}, dimensions={0} | all-to-all | bytes 33554432 | tf_op jit(solution)/shard_map/all_to_all | solution.py:15
  979.6 16.5 %fusion.6 = bf16[512,2048]{1,0:T(8,128)(2,1)} fusion(bf16[2048,4096]{1,0:T(8,128)(2,1)} %bitcast.180, bf16[512,2048]{1,0:T(8,128)(2,1)} %bitcast.75), kind=kOutput, calls=%fused_computation.8 | convolution fusion | flops 8594128896 | bytes 20971520 | tf_op jit(solution)/shard_map/dot_general | solution.py:199
  996.0 29.7 %all_to_all.21 = bf16[4,128,2048]{2,1,0:T(8,128)(2,1)S(1)} all-to-all(bf16[4,128,2048]{2,1,0:T(8,128)(2,1)} %bitcast.182), channel_id=1, replica_groups=mesh['grp'=2,'sp_0'=16,'sp_1'=2,'tp'=4] {'tp'}, dimensions={0} | all-to-all | bytes 4194304 | tf_op jit(solution)/shard_map/all_to_all | solution.py:63
  1025.7 0.4 convert_reduce_fusion
  1026.1 0.9 fusion.24
  (36 shorter events, 0.1 us)
Async XLA Ops:
  6.5 175.6 %copy-start = (bf16[512,2048]{1,0:T(8,128)(2,1)S(1)}, bf16[512,2048]{1,0:T(8,128)(2,1)}, u32[]{:S(2)}) copy-start(bf16[512,2048]{1,0:T(8,128)(2,1)} %param.27) | copy-start | bytes 6291460
  6.6 99.3 %copy-start.4 = (bf16[512,256]{1,0:T(8,128)(2,1)S(1)}, bf16[512,256]{1,0:T(8,128)(2,1)}, u32[]{:S(2)}) copy-start(bf16[512,256]{1,0:T(8,128)(2,1)} %param.22) | copy-start | bytes 786436
  6.6 99.3 %copy-start.7 = (bf16[512,128]{1,0:T(8,128)(2,1)S(1)}, bf16[512,128]{1,0:T(8,128)(2,1)}, u32[]{:S(2)}) copy-start(bf16[512,128]{1,0:T(8,128)(2,1)} %param.21) | copy-start | bytes 393220
  6.6 101.6 %copy-start.11 = (bf16[512,256]{1,0:T(8,128)(2,1)S(1)}, bf16[512,256]{1,0:T(8,128)(2,1)}, u32[]{:S(2)}) copy-start(bf16[512,256]{1,0:T(8,128)(2,1)} %param.18) | copy-start | bytes 786436
  6.6 104.5 %all-gather.9.cloned.1.call-start = ((), (), s32[]{:S(2)}) async-start(), calls=%async_computation.5 | async-start | bytes 1114112 | tf_op jit(solution)/shard_map/all_gather | solution.py:30
  45.8 130.1 %all-gather.7.cloned.1.call-start = ((), (), s32[]{:S(2)}) async-start(), calls=%async_computation.4 | async-start | bytes 4456448 | tf_op jit(solution)/shard_map/all_gather | solution.py:30
  108.1 6.1 copy-start.9
  111.1 3.2 copy-start.3
  114.2 61.7 %copy-start.12 = (bf16[512,256]{1,0:T(8,128)(2,1)S(1)}, bf16[512,256]{1,0:T(8,128)(2,1)}, u32[]{:S(2)}) copy-start(bf16[512,256]{1,0:T(8,128)(2,1)} %param.17) | copy-start | bytes 786436
  175.9 6.2 copy-start.2
  175.9 6.2 copy-start.10
  185.0 22.0 %copy-start.8 = (f32[2048]{0:T(1024)S(1)}, f32[2048]{0:T(1024)}, u32[]{:S(2)}) copy-start(f32[2048]{0:T(1024)} %param.29) | copy-start | bytes 24580
  185.0 20.3 %all-to-all-start = ((bf16[4,128,2048]{2,1,0:T(8,128)(2,1)}), bf16[4,128,2048]{2,1,0:T(8,128)(2,1)S(1)}, u32[]{:S(2)}, u32[]{:S(2)}) async-start(bf16[4,128,2048]{2,1,0:T(8,128)(2,1)} %bitcast.181), calls=%async_computation | async-start | bytes 4194304 | tf_op jit(solution)/shard_map/all_to_all | solution.py:63
  207.0 6.4 copy-start.5
  207.0 6.4 copy-start.6
  208.9 19.9 %all-to-all-start.1 = ((bf16[4,128,2048]{2,1,0:T(8,128)(2,1)}), bf16[4,128,2048]{2,1,0:T(8,128)(2,1)}, u32[]{:S(2)}, u32[]{:S(2)}) async-start(bf16[4,128,2048]{2,1,0:T(8,128)(2,1)} %broadcast_in_dim.16), calls=%async_computation.1 | async-start | bytes 4194304 | tf_op jit(solution)/shard_map/all_to_all | solution.py:75
  996.0 31.0 %copy-start.1 = (bf16[512,2048]{1,0:T(8,128)(2,1)S(1)}, bf16[512,2048]{1,0:T(8,128)(2,1)}, u32[]{:S(2)}) copy-start(bf16[512,2048]{1,0:T(8,128)(2,1)} %param.27) | copy-start | bytes 6291460
Sparse Core Ops, SparseCore 0:
  45.9 53.1 all-gather.8
  100.9 74.9 all-gather.6
